TPU v7x, 32 devices: a whole 2x2x4 slice. The times are simulated.
32 devices in a mesh: sp: 4 (over y, x), tp: 8 (over z, core).
Axes of the slice: x: 2, y: 2, z: 4, core: 2. Of those that a mesh axis runs over, the one named last changes fastest.
Arguments:
- tokens: bfloat16 [2048, 4096], P('sp', 'tp'), may hold values from -6 to 6
- pre_gain: float32 [2, 4096], replicated, may hold values from 0.1 to 1.9
- w_value: bfloat16 [2, 4096, 4096], P(None, 'sp', 'tp'), may hold values from -0.09375 to 0.09375
- w_gate: bfloat16 [2, 4096, 4096], P(None, 'sp', 'tp'), may hold values from -0.09375 to 0.09375
- conv_taps: float32 [2, 31, 4096], P(None, None, 'tp'), may hold values from -3.5 to 3.5
- conv_bias: float32 [2, 4096], P(None, 'tp'), may hold values from -3 to 3
- norm_gain: float32 [2, 4096], P(None, 'tp'), may hold values from 0.1 to 1.9
- norm_bias: float32 [2, 4096], P(None, 'tp'), may hold values from -3 to 3
- w_out: bfloat16 [2, 4096, 4096], P(None, 'sp', 'tp'), may hold values from -0.09375 to 0.09375
- post_gain: float32 [2, 4096], P(None, 'tp'), may hold values from 0.1 to 1.9
Outputs:
- stream: bfloat16 [2048, 4096], P('sp', 'tp')
All inputs are finite; a program needn't handle non-finite values.
Results may differ from a plain program's by a relative error of at most 0.009.
Values may be sent and summed in bfloat16 or wider, within the bound.
A program may use at most 64 MiB of HBM per device.

v0:
```python
import jax
import jax.numpy as jnp
from jax import lax
from jax.sharding import PartitionSpec as P


def passed_along(value, axis, steps):
    count = lax.axis_size(axis)
    leading, last = (max(0, -steps), min(count, count - steps))
    return lax.ppermute(value, axis, [(source, source + steps) for source in range(leading, last)])


def shards(
    tokens, pre_gain, w_value, w_gate, conv_taps, conv_bias, norm_gain, norm_bias, w_out, post_gain
):
    layer_count = w_value.shape[0]
    tap_count = conv_taps.shape[1]
    channel_count = conv_taps.shape[2] * lax.axis_size("tp")
    model_width = tokens.shape[1] * lax.axis_size("tp")
    local_rows = tokens.shape[0]
    every_value, every_gate, every_out = (
        lax.all_gather(w_value, "sp", axis=1, tiled=True),
        lax.all_gather(w_gate, "sp", axis=1, tiled=True),
        lax.all_gather(w_out, "sp", axis=1, tiled=True),
    )
    stream = tokens
    for layer_index in range(layer_count):
        gathered = lax.all_gather(stream, "tp", axis=1, tiled=True)
        full_rows = gathered.astype(jnp.float32)
        scale_rows = lax.rsqrt(jnp.mean(full_rows * full_rows, axis=-1, keepdims=True) + 1e-06)
        normed = (full_rows * scale_rows * pre_gain[layer_index]).astype(jnp.bfloat16)
        value_block = every_value[layer_index]
        gate_block = every_gate[layer_index]
        out_block = every_out[layer_index]
        value_proj = jnp.dot(normed, value_block, preferred_element_type=jnp.float32)
        gate_proj = jnp.dot(normed, gate_block, preferred_element_type=jnp.float32)
        glu_out = (value_proj * jax.nn.sigmoid(gate_proj)).astype(jnp.bfloat16)
        earlier = passed_along(glu_out[local_rows - (tap_count - 1) :], "sp", 1)
        padded = jnp.concatenate([earlier, glu_out], axis=0).astype(jnp.float32)
        filtered = jnp.zeros(glu_out.shape, jnp.float32) + conv_bias[layer_index]
        for tap_index in range(tap_count):
            filtered = (
                filtered
                + padded[tap_index : tap_index + local_rows] * conv_taps[layer_index, tap_index]
            )
        channel_sum, channel_square = lax.psum(
            (jnp.sum(filtered, axis=-1), jnp.sum(filtered * filtered, axis=-1)), "tp"
        )
        centre = channel_sum / channel_count
        spread = jnp.maximum(channel_square / channel_count - centre * centre, 0.0)
        shaped = (filtered - centre[:, None]) * lax.rsqrt(spread + 1e-05)[:, None]
        mixed = jax.nn.silu(shaped * norm_gain[layer_index] + norm_bias[layer_index]).astype(
            jnp.bfloat16
        )
        whole_mixed = lax.all_gather(mixed, "tp", axis=1, tiled=True)
        branch_low = jnp.dot(whole_mixed, out_block, preferred_element_type=jnp.float32).astype(
            jnp.bfloat16
        )
        branch = lax.optimization_barrier(branch_low).astype(jnp.float32)
        total = lax.psum(jnp.sum(branch * branch, axis=-1), "tp")
        rescale = lax.rsqrt(total / model_width + 1e-06)[:, None]
        stream = (stream.astype(jnp.float32) + branch * rescale * post_gain[layer_index]).astype(
            jnp.bfloat16
        )
    return stream


def solution(mesh):
    in_specs = (
        P("sp", "tp"),
        P(),
        P(None, "sp", "tp"),
        P(None, "sp", "tp"),
        P(None, None, "tp"),
        P(None, "tp"),
        P(None, "tp"),
        P(None, "tp"),
        P(None, "sp", "tp"),
        P(None, "tp"),
    )
    out_specs = P("sp", "tp")
    return jax.shard_map(shards, mesh=mesh, in_specs=in_specs, out_specs=out_specs, check_vma=False)
```

profile of v0, /device:TPU:0, one launch (start us, length us, event | category | flops | bytes accessed | tf_op | source)
XLA Modules:
  0.0 551.2 jit_solution(2232420375245703278)
XLA Ops:
  9.6 49.0 %all-gather.8.cloned.1.call-done = bf16[512,4096]{1,0:T(8,128)(2,1)} async-done(((bf16[512,512]{1,0:T(8,128)(2,1)}), bf16[512,4096]{1,0:T(8,128)(2,1)}) %all-gather.8.cloned.1.call-update) | async-done | bytes 4194320 | tf_op jit(solution)/shard_map/all_gather | solution.py:28
  58.6 3.1 fusion
  61.7 85.1 %all-gather.12.cloned.1.call-done = bf16[2,4096,512]{2,1,0:T(8,128)(2,1)} async-done(((bf16[2,1024,512]{2,1,0:T(8,128)(2,1)}), bf16[2,4096,512]{2,1,0:T(8,128)(2,1)}) %all-gather.12.cloned.1.call-update) | async-done | bytes 8388624 | tf_op jit(solution)/shard_map/all_gather | solution.py:23
  146.7 6.0 %fusion.21 = f32[512,512]{1,0:T(8,128)S(1)} fusion(bf16[2,4096,512]{2,1,0:T(8,128)(2,1)} %all-gather.12.cloned.1.call-done, bf16[512,4096]{1,0:T(8,128)(2,1)} %all-gather.8.cloned.1.call-done, f32[4096]{0:T(1024)S(1)} %bitcast.122, f32[512]{0:T(512)S(1)} %add_rsqrt_fusion.5), kind=kOutput, calls=%fused_computation.35 | convolution fusion | flops 2156658688 | bytes 9455616 | tf_op jit(solution)/shard_map/dot_general | solution.py:36
  152.7 83.4 %all-gather.10.cloned.1.call-done = bf16[2,4096,512]{2,1,0:T(8,128)(2,1)} async-done(((bf16[2,1024,512]{2,1,0:T(8,128)(2,1)}), bf16[2,4096,512]{2,1,0:T(8,128)(2,1)}) %all-gather.10.cloned.1.call-update) | async-done | bytes 8388624 | tf_op jit(solution)/shard_map/all_gather | solution.py:22
  236.1 5.8 %fusion.23 = bf16[512,512]{1,0:T(8,128)(2,1)S(1)} fusion(f32[512,512]{1,0:T(8,128)S(1)} %fusion.21, bf16[2,4096,512]{2,1,0:T(8,128)(2,1)} %all-gather.10.cloned.1.call-done, bf16[512,4096]{1,0:T(8,128)(2,1)} %all-gather.8.cloned.1.call-done, f32[4096]{0:T(1024)S(1)} %bitcast.123, f32[512]{0:T(512)S(1)} %add_rsqrt_fusion.5), kind=kOutput, calls=%fused_computation.37 | convolution fusion | flops 2156396544 | bytes 9979904 | tf_op jit(solution)/shard_map/dot_general | solution.py:35
  242.0 3.4 collective-permute-start
  245.4 1.6 collective-permute-done
  247.1 5.0 fusion.101
  252.1 15.3 %all-reduce.1 = (f32[512]{0:T(512)S(1)}, f32[512]{0:T(512)S(1)}) all-reduce(f32[512]{0:T(512)S(1)} %get-tuple-element.8, f32[512]{0:T(512)S(1)} %get-tuple-element.7), channel_id=1, replica_groups=mesh['sp'=4,'tp'=8] {'tp'}, use_global_device_ids=true, to_apply=%region_4.0 | all-reduce | flops 1024 | bytes 8192 | tf_op jit(solution)/shard_map/psum | solution.py:46
  268.8 56.5 %all-gather.16.cloned.1.call-done = bf16[2,4096,512]{2,1,0:T(8,128)(2,1)} async-done(((bf16[2,1024,512]{2,1,0:T(8,128)(2,1)}), bf16[2,4096,512]{2,1,0:T(8,128)(2,1)}) %all-gather.16.cloned.1.call-update) | async-done | bytes 8388624 | tf_op jit(solution)/shard_map/all_gather | solution.py:24
  325.3 48.4 %all-gather.14.cloned.1.call-done = bf16[512,4096]{1,0:T(8,128)(2,1)} async-done(((bf16[512,512]{1,0:T(8,128)(2,1)}), bf16[512,4096]{1,0:T(8,128)(2,1)}) %all-gather.14.cloned.1.call-update) | async-done | bytes 4194320 | tf_op jit(solution)/shard_map/all_gather | solution.py:55
  373.7 5.8 %fusion.24 = bf16[512,512]{1,0:T(8,128)(2,1)S(1)} fusion(bf16[512,4096]{1,0:T(8,128)(2,1)} %all-gather.14.cloned.1.call-done, bf16[2,4096,512]{2,1,0:T(8,128)(2,1)} %all-gather.16.cloned.1.call-done), kind=kOutput, calls=%fused_computation.38 | convolution fusion | flops 2147745792 | bytes 8912896 | tf_op jit(solution)/shard_map/dot_general | solution.py:56
  379.6 14.8 %psum.44 = f32[512]{0:T(512)S(1)} all-reduce(f32[512]{0:T(512)S(1)} %fusion.30), channel_id=1, replica_groups=mesh['sp'=4,'tp'=8] {'tp'}, use_global_device_ids=true, to_apply=%region_6.7 | all-reduce | flops 512 | bytes 4096 | tf_op jit(solution)/shard_map/psum | solution.py:60
  395.8 44.7 %all-gather.18.cloned.1.call-done = bf16[512,4096]{1,0:T(8,128)(2,1)} async-done(((bf16[512,512]{1,0:T(8,128)(2,1)}), bf16[512,4096]{1,0:T(8,128)(2,1)}) %all-gather.18.cloned.1.call-update) | async-done | bytes 4194320 | tf_op jit(solution)/shard_map/all_gather | solution.py:28
  440.5 3.2 fusion.3
  443.9 5.0 fusion.19
  449.0 2.4 fusion.22
  451.4 3.4 collective-permute-start.1
  456.5 5.0 fusion.100
  461.6 13.7 %all-reduce = (f32[512]{0:T(512)S(1)}, f32[512]{0:T(512)S(1)}) all-reduce(f32[512]{0:T(512)S(1)} %get-tuple-element.6, f32[512]{0:T(512)S(1)} %get-tuple-element.5), channel_id=1, replica_groups=mesh['sp'=4,'tp'=8] {'tp'}, use_global_device_ids=true, to_apply=%region_11.12 | all-reduce | flops 1024 | bytes 8192 | tf_op jit(solution)/shard_map/psum | solution.py:46
  476.6 45.9 %all-gather.20.cloned.1.call-done = bf16[512,4096]{1,0:T(8,128)(2,1)} async-done(((bf16[512,512]{1,0:T(8,128)(2,1)}), bf16[512,4096]{1,0:T(8,128)(2,1)}) %all-gather.20.cloned.1.call-update) | async-done | bytes 4194320 | tf_op jit(solution)/shard_map/all_gather | solution.py:55
  522.5 5.8 %fusion.25 = bf16[512,512]{1,0:T(8,128)(2,1)S(1)} fusion(bf16[512,4096]{1,0:T(8,128)(2,1)} %all-gather.20.cloned.1.call-done, bf16[2,4096,512]{2,1,0:T(8,128)(2,1)} %all-gather.16.cloned.1.call-done), kind=kOutput, calls=%fused_computation.39 | convolution fusion | flops 2147745792 | bytes 8912896 | tf_op jit(solution)/shard_map/dot_general | solution.py:56
  528.5 14.8 %psum.47 = f32[512]{0:T(512)S(1)} all-reduce(f32[512]{0:T(512)S(1)} %fusion.34), channel_id=1, replica_groups=mesh['sp'=4,'tp'=8] {'tp'}, use_global_device_ids=true, to_apply=%region_13.14 | all-reduce | flops 512 | bytes 4096 | tf_op jit(solution)/shard_map/psum | solution.py:60
  (63 shorter events, 10.4 us)
Async XLA Ops:
  6.5 2.8 copy-start.5
  6.5 2.9 copy-start.6
  6.5 2.9 copy-start.3
  6.5 3.0 copy-start.4
  6.5 52.0 %all-gather.8.cloned.1.call-start = ((), (), s32[]{:S(2)}) async-start(), calls=%async_computation | async-start | bytes 4718592 | tf_op jit(solution)/shard_map/all_gather | solution.py:28
  7.3 139.5 %all-gather.12.cloned.1.call-start = ((), (), s32[]{:S(2)}) async-start(), calls=%async_computation.2 | async-start | bytes 10485760 | tf_op jit(solution)/shard_map/all_gather | solution.py:23
  8.0 228.1 %all-gather.10.cloned.1.call-start = ((), (), s32[]{:S(2)}) async-start(), calls=%async_computation.1 | async-start | bytes 10485760 | tf_op jit(solution)/shard_map/all_gather | solution.py:22
  8.8 316.6 %all-gather.16.cloned.1.call-start = ((), (), s32[]{:S(2)}) async-start(), calls=%async_computation.4 | async-start | bytes 10485760 | tf_op jit(solution)/shard_map/all_gather | solution.py:24
  9.3 364.3 %all-gather.14.cloned.1.call-start = ((), (), s32[]{:S(2)}) async-start(), calls=%async_computation.3 | async-start | bytes 4718592 | tf_op jit(solution)/shard_map/all_gather | solution.py:55
  152.7 92.6 %copy-start.7 = (f32[2,512]{1,0:T(2,128)S(1)}, f32[2,512]{1,0:T(2,128)}, u32[]{:S(2)}) copy-start(f32[2,512]{1,0:T(2,128)} %param.16) | copy-start | bytes 12292
  242.0 5.0 collective-permute-start
  247.1 21.7 %copy-start.8 = (f32[2,512]{1,0:T(2,128)S(1)}, f32[2,512]{1,0:T(2,128)}, u32[]{:S(2)}) copy-start(f32[2,512]{1,0:T(2,128)} %param.19) | copy-start | bytes 12292
  268.7 171.8 %all-gather.18.cloned.1.call-start = ((), (), s32[]{:S(2)}) async-start(), calls=%async_computation.5 | async-start | bytes 4718592 | tf_op jit(solution)/shard_map/all_gather | solution.py:28
  268.8 125.7 %copy-start.2 = (bf16[512,512]{1,0:T(8,128)(2,1)S(1)}, bf16[512,512]{1,0:T(8,128)(2,1)}, u32[]{:S(2)}) copy-start(bf16[512,512]{1,0:T(8,128)(2,1)} %param.10) | copy-start | bytes 1572868
  395.5 127.0 %all-gather.20.cloned.1.call-start = ((), (), s32[]{:S(2)}) async-start(), calls=%async_computation.6 | async-start | bytes 4718592 | tf_op jit(solution)/shard_map/all_gather | solution.py:55
  440.5 3.4 copy-start.1
  440.5 8.5 %slice-start = ((s8[8388608]{0:T(1024)(128)(4,1)}), s8[4194304]{0:T(1024)(128)(4,1)S(1)}, s32[]{:S(2)}) async-start(s8[8388608]{0:T(1024)(128)(4,1)} %bitcast.194), calls=%async_computation.7 | async-start | bytes 8388608
  443.9 5.0 slice-start.1
  451.4 5.0 collective-permute-start.1
  476.6 66.7 %copy-start = (bf16[512,512]{1,0:T(8,128)(2,1)S(1)}, bf16[512,512]{1,0:T(8,128)(2,1)}, u32[]{:S(2)}) copy-start(bf16[512,512]{1,0:T(8,128)(2,1)} %fusion.33) | copy-start | bytes 1572868
Sparse Core Ops, SparseCore 0:
  9.0 49.5 all-gather.7
  60.4 86.2 all-gather.11
  148.6 87.4 all-gather.9
  237.8 87.4 all-gather.15
  326.8 46.8 all-gather.13
  395.7 44.7 all-gather.17
  476.7 45.7 all-gather.19
where the time goes:
time: 551 us
  waiting for transfers between devices  419 us (76%)
  blocking collectives  58.7 us (11%)
  matrix products  30.8 us (6%)
  other arithmetic  21.7 us (4%)
  between operations  13.8 us (3%)
  starting transfers between devices  7.2 us (1%)
    all_gather x2, waiting for transfers between devices, shards(): whole_mixed = lax.all_gather(mixed, 'tp', axis=1, tiled=True)  94.2 us
    all_gather x2, waiting for transfers between devices, shards(): gathered = lax.all_gather(stream, 'tp', axis=1, tiled=True)  93.7 us
    all_gather x1, waiting for transfers between devices, shards(): lax.all_gather(w_gate, 'sp', axis=1, tiled=True)  85.1 us
    all_gather x1, waiting for transfers between devices, shards(): lax.all_gather(w_value, 'sp', axis=1, tiled=True)  83.4 us
    all_gather x1, waiting for transfers between devices, shards(): lax.all_gather(w_out, 'sp', axis=1, tiled=True)  56.5 us
    psum x2, blocking collectives, shards(): total = lax.psum(jnp.sum(branch * branch, axis=-1), 'tp')  29.6 us
    psum x2, blocking collectives, shards(): lax.psum((jnp.sum(filtered, axis=-1), jnp.sum(filtered * filtered, axis=-...  29.1 us
    dot_general x2, matrix products, shards(): jnp.dot(whole_mixed, out_block, preferred_element_type=jnp.float32)  11.6 us
  transfers between devices with their start and end apart: 9, of which 9 were waited for; matrix products, arithmetic and copies ran while one was open for 4% of the time, Pallas kernels for 0%

commit v1 on v0

--- a/solution.py
+++ b/solution.py
@@ -2,6 +2,10 @@
 import jax.numpy as jnp
 from jax import lax
 from jax.sharding import PartitionSpec as P
+
+
+def take_the_stacks_all(page, row_dim):
+    return jnp.concatenate(lax.all_gather(page, "tp"), row_dim)
 
 
 def passed_along(value, axis, steps):
@@ -25,7 +29,7 @@
     )
     stream = tokens
     for layer_index in range(layer_count):
-        gathered = lax.all_gather(stream, "tp", axis=1, tiled=True)
+        gathered = take_the_stacks_all(stream, 1)
         full_rows = gathered.astype(jnp.float32)
         scale_rows = lax.rsqrt(jnp.mean(full_rows * full_rows, axis=-1, keepdims=True) + 1e-06)
         normed = (full_rows * scale_rows * pre_gain[layer_index]).astype(jnp.bfloat16)

time: 551 us -> 569 us (1.033)
  local copies, waits for them, and re-layouts: 0.46 us -> 16.7 us
  other arithmetic: 21.7 us -> 33.5 us
  waiting for transfers between devices: 419 us -> 408 us
    convert_element_type x0 -> x2, local copies, waits for them, and re-layouts: none -> 16 us  [the longest x1 9.11 us: shards(): full_rows = gathered.astype(jnp.float32)]
    convert_element_type x0 -> x3, other arithmetic: none -> 11.7 us  [the longest x2 7.35 us: shards(): (full_rows * scale_rows * pre_gain[layer_index]).astype(jnp.bfloat16)]
    all_gather x1, waiting for transfers between devices: 85.1 us -> 74.6 us  [shards(): lax.all_gather(w_gate, 'sp', axis=1, tiled=True)]
  transfers between devices with their start and end apart: 9 -> 9, of which waited for: 9 -> 9; matrix products, arithmetic and copies ran while one was open for 4% -> 6% of each run, Pallas kernels for 0% -> 0%
where the time goes in v1:
time: 569 us; the launch traced here: 568 us
  waiting for transfers between devices  408 us (72%)
  blocking collectives  58.7 us (10%)
  other arithmetic  33.5 us (6%)
  matrix products  30.5 us (5%)
  local copies, waits for them, and re-layouts  16.7 us (3%)
  between operations  13.8 us (2%)
  starting transfers between devices  7.2 us (1%)
    all_gather x2, waiting for transfers between devices, shards(): whole_mixed = lax.all_gather(mixed, 'tp', axis=1, tiled=True)  94.2 us
    all_gather x2, waiting for transfers between devices, take_the_stacks_all(): return jnp.concatenate(lax.all_gather(page, 'tp'), row_dim)  93.6 us
    all_gather x1, waiting for transfers between devices, shards(): lax.all_gather(w_value, 'sp', axis=1, tiled=True)  83.4 us
    all_gather x1, waiting for transfers between devices, shards(): lax.all_gather(w_gate, 'sp', axis=1, tiled=True)  74.6 us
    all_gather x1, waiting for transfers between devices, shards(): lax.all_gather(w_out, 'sp', axis=1, tiled=True)  56.6 us
    psum x2, blocking collectives, shards(): total = lax.psum(jnp.sum(branch * branch, axis=-1), 'tp')  29.6 us
    psum x2, blocking collectives, shards(): lax.psum((jnp.sum(filtered, axis=-1), jnp.sum(filtered * filtered, axis=-...  29.1 us
    dot_general x2, matrix products, shards(): jnp.dot(whole_mixed, out_block, preferred_element_type=jnp.float32)  11.6 us
  transfers between devices with their start and end apart: 9, of which 9 were waited for; matrix products, arithmetic and copies ran while one was open for 6% of the time, Pallas kernels for 0%

profile of v1, /device:TPU:0, one launch (start us, length us, event | category | flops | bytes accessed | tf_op | source)
XLA Modules:
  0.0 568.5 jit_solution(5599667281327966905)
XLA Ops:
  9.7 48.9 %all-gather.20.cloned.1.call-done = bf16[4096,512]{1,0:T(8,128)(2,1)} async-done(((bf16[512,512]{1,0:T(8,128)(2,1)}), bf16[4096,512]{1,0:T(8,128)(2,1)}) %all-gather.20.cloned.1.call-update) | async-done | bytes 4194320 | tf_op jit(solution)/shard_map/all_gather | solution.py:8
  65.3 6.8 %copy.12 = bf16[512,8,512]{0,2,1:T(8,128)(2,1)} copy(bf16[512,8,512]{2,0,1:T(8,128)(2,1)} %fusion.3) | data formatting | bytes 8388608 | tf_op jit(solution)/shard_map/convert_element_type | solution.py:35
  72.1 74.6 %all-gather.12.cloned.1.call-done = bf16[2,4096,512]{2,1,0:T(8,128)(2,1)} async-done(((bf16[2,1024,512]{2,1,0:T(8,128)(2,1)}), bf16[2,4096,512]{2,1,0:T(8,128)(2,1)}) %all-gather.12.cloned.1.call-update) | async-done | bytes 8388624 | tf_op jit(solution)/shard_map/all_gather | solution.py:27
  146.7 6.0 %fusion.19 = f32[512,512]{1,0:T(8,128)S(1)} fusion(bf16[512,4096]{0,1:T(8,128)(2,1)} %bitcast.136, bf16[2,4096,512]{2,1,0:T(8,128)(2,1)} %all-gather.12.cloned.1.call-done), kind=kOutput, calls=%fused_computation.33 | convolution fusion | flops 2148270080 | bytes 9437184 | tf_op jit(solution)/shard_map/dot_general | solution.py:40
  152.7 83.4 %all-gather.10.cloned.1.call-done = bf16[2,4096,512]{2,1,0:T(8,128)(2,1)} async-done(((bf16[2,1024,512]{2,1,0:T(8,128)(2,1)}), bf16[2,4096,512]{2,1,0:T(8,128)(2,1)}) %all-gather.10.cloned.1.call-update) | async-done | bytes 8388624 | tf_op jit(solution)/shard_map/all_gather | solution.py:26
  236.1 5.8 %fusion.21 = bf16[512,512]{1,0:T(8,128)(2,1)S(1)} fusion(f32[512,512]{1,0:T(8,128)S(1)} %fusion.19, bf16[512,4096]{0,1:T(8,128)(2,1)} %bitcast.137, bf16[2,4096,512]{2,1,0:T(8,128)(2,1)} %all-gather.10.cloned.1.call-done), kind=kOutput, calls=%fused_computation.35 | convolution fusion | flops 2148007936 | bytes 9961472 | tf_op jit(solution)/shard_map/dot_general | solution.py:39
  241.9 3.4 collective-permute-start
  247.1 5.0 fusion.95
  252.1 15.3 %all-reduce.1 = (f32[512]{0:T(512)S(1)}, f32[512]{0:T(512)S(1)}) all-reduce(f32[512]{0:T(512)S(1)} %get-tuple-element.8, f32[512]{0:T(512)S(1)} %get-tuple-element.7), channel_id=1, replica_groups=mesh['sp'=4,'tp'=8] {'tp'}, use_global_device_ids=true, to_apply=%region_4.0 | all-reduce | flops 1024 | bytes 8192 | tf_op jit(solution)/shard_map/psum | solution.py:50
  268.7 56.6 %all-gather.16.cloned.1.call-done = bf16[2,4096,512]{2,1,0:T(8,128)(2,1)} async-done(((bf16[2,1024,512]{2,1,0:T(8,128)(2,1)}), bf16[2,4096,512]{2,1,0:T(8,128)(2,1)}) %all-gather.16.cloned.1.call-update) | async-done | bytes 8388624 | tf_op jit(solution)/shard_map/all_gather | solution.py:28
  325.3 48.4 %all-gather.14.cloned.1.call-done = bf16[512,4096]{1,0:T(8,128)(2,1)} async-done(((bf16[512,512]{1,0:T(8,128)(2,1)}), bf16[512,4096]{1,0:T(8,128)(2,1)}) %all-gather.14.cloned.1.call-update) | async-done | bytes 4194320 | tf_op jit(solution)/shard_map/all_gather | solution.py:59
  373.7 5.8 %fusion.22 = bf16[512,512]{1,0:T(8,128)(2,1)S(1)} fusion(bf16[512,4096]{1,0:T(8,128)(2,1)} %all-gather.14.cloned.1.call-done, bf16[2,4096,512]{2,1,0:T(8,128)(2,1)} %all-gather.16.cloned.1.call-done), kind=kOutput, calls=%fused_computation.36 | convolution fusion | flops 2147745792 | bytes 8912896 | tf_op jit(solution)/shard_map/dot_general | solution.py:60
  379.6 14.8 %psum.44 = f32[512]{0:T(512)S(1)} all-reduce(f32[512]{0:T(512)S(1)} %fusion.24), channel_id=1, replica_groups=mesh['sp'=4,'tp'=8] {'tp'}, use_global_device_ids=true, to_apply=%region_6.7 | all-reduce | flops 512 | bytes 4096 | tf_op jit(solution)/shard_map/psum | solution.py:64
  395.8 44.7 %all-gather.22.cloned.1.call-done = bf16[4096,512]{1,0:T(8,128)(2,1)} async-done(((bf16[512,512]{1,0:T(8,128)(2,1)}), bf16[4096,512]{1,0:T(8,128)(2,1)}) %all-gather.22.cloned.1.call-update) | async-done | bytes 4194320 | tf_op jit(solution)/shard_map/all_gather | solution.py:8
  443.9 4.4 bitcast_convert_fusion
  448.3 9.1 %copy.13 = f32[8,512,512]{1,2,0:T(8,128)} copy(f32[8,512,512]{2,1,0:T(8,128)} %bitcast_convert_fusion) | data formatting | bytes 16777216 | tf_op jit(solution)/shard_map/convert_element_type | solution.py:33
  457.4 4.1 multiply_convert_fusion
  461.5 4.8 fusion.17
  468.7 3.4 collective-permute-start.1
  473.9 5.0 fusion.94
  478.9 13.7 %all-reduce = (f32[512]{0:T(512)S(1)}, f32[512]{0:T(512)S(1)}) all-reduce(f32[512]{0:T(512)S(1)} %get-tuple-element.6, f32[512]{0:T(512)S(1)} %get-tuple-element.5), channel_id=1, replica_groups=mesh['sp'=4,'tp'=8] {'tp'}, use_global_device_ids=true, to_apply=%region_11.12 | all-reduce | flops 1024 | bytes 8192 | tf_op jit(solution)/shard_map/psum | solution.py:50
  493.9 45.9 %all-gather.18.cloned.1.call-done = bf16[512,4096]{1,0:T(8,128)(2,1)} async-done(((bf16[512,512]{1,0:T(8,128)(2,1)}), bf16[512,4096]{1,0:T(8,128)(2,1)}) %all-gather.18.cloned.1.call-update) | async-done | bytes 4194320 | tf_op jit(solution)/shard_map/all_gather | solution.py:59
  539.8 5.8 %fusion.23 = bf16[512,512]{1,0:T(8,128)(2,1)S(1)} fusion(bf16[512,4096]{1,0:T(8,128)(2,1)} %all-gather.18.cloned.1.call-done, bf16[2,4096,512]{2,1,0:T(8,128)(2,1)} %all-gather.16.cloned.1.call-done), kind=kOutput, calls=%fused_computation.37 | convolution fusion | flops 2147745792 | bytes 8912896 | tf_op jit(solution)/shard_map/dot_general | solution.py:60
  545.7 14.8 %psum.47 = f32[512]{0:T(512)S(1)} all-reduce(f32[512]{0:T(512)S(1)} %fusion.28), channel_id=1, replica_groups=mesh['sp'=4,'tp'=8] {'tp'}, use_global_device_ids=true, to_apply=%region_13.14 | all-reduce | flops 512 | bytes 4096 | tf_op jit(solution)/shard_map/psum | solution.py:64
  (72 shorter events, 24.3 us)
Async XLA Ops:
  6.5 2.8 copy-start.5
  6.5 3.0 copy-start.6
  6.5 3.0 copy-start.7
  6.5 3.0 copy-start.4
  6.5 52.0 %all-gather.20.cloned.1.call-start = ((), (), s32[]{:S(2)}) async-start(), calls=%async_computation.5 | async-start | bytes 4718592 | tf_op jit(solution)/shard_map/all_gather | solution.py:8
  7.3 139.5 %all-gather.12.cloned.1.call-start = ((), (), s32[]{:S(2)}) async-start(), calls=%async_computation.1 | async-start | bytes 10485760 | tf_op jit(solution)/shard_map/all_gather | solution.py:27
  8.0 228.1 %all-gather.10.cloned.1.call-start = ((), (), s32[]{:S(2)}) async-start(), calls=%async_computation | async-start | bytes 10485760 | tf_op jit(solution)/shard_map/all_gather | solution.py:26
  8.8 316.5 %all-gather.16.cloned.1.call-start = ((), (), s32[]{:S(2)}) async-start(), calls=%async_computation.3 | async-start | bytes 10485760 | tf_op jit(solution)/shard_map/all_gather | solution.py:28
  9.3 364.3 %all-gather.14.cloned.1.call-start = ((), (), s32[]{:S(2)}) async-start(), calls=%async_computation.2 | async-start | bytes 4718592 | tf_op jit(solution)/shard_map/all_gather | solution.py:59
  58.6 3.4 copy-start.1
  152.7 92.6 %copy-start.8 = (f32[2,512]{1,0:T(2,128)S(1)}, f32[2,512]{1,0:T(2,128)}, u32[]{:S(2)}) copy-start(f32[2,512]{1,0:T(2,128)} %param.17) | copy-start | bytes 12292
  241.9 5.0 collective-permute-start
  247.1 21.7 %copy-start.9 = (f32[2,512]{1,0:T(2,128)S(1)}, f32[2,512]{1,0:T(2,128)}, u32[]{:S(2)}) copy-start(f32[2,512]{1,0:T(2,128)} %param.19) | copy-start | bytes 12292
  268.7 171.8 %all-gather.22.cloned.1.call-start = ((), (), s32[]{:S(2)}) async-start(), calls=%async_computation.6 | async-start | bytes 4718592 | tf_op jit(solution)/shard_map/all_gather | solution.py:8
  268.7 125.7 %copy-start.3 = (bf16[512,512]{1,0:T(8,128)(2,1)S(1)}, bf16[512,512]{1,0:T(8,128)(2,1)}, u32[]{:S(2)}) copy-start(bf16[512,512]{1,0:T(8,128)(2,1)} %param.10) | copy-start | bytes 1572868
  395.5 144.2 %all-gather.18.cloned.1.call-start = ((), (), s32[]{:S(2)}) async-start(), calls=%async_computation.4 | async-start | bytes 4718592 | tf_op jit(solution)/shard_map/all_gather | solution.py:59
  440.5 3.4 copy-start
  457.4 8.9 %slice-start = ((s8[8388608]{0:T(1024)(128)(4,1)}), s8[4194304]{0:T(1024)(128)(4,1)S(1)}, s32[]{:S(2)}) async-start(s8[8388608]{0:T(1024)(128)(4,1)} %bitcast.210), calls=%async_computation.7 | async-start | bytes 8388608
  461.5 4.9 slice-start.1
  468.7 5.0 collective-permute-start.1
  493.9 66.7 %copy-start.2 = (bf16[512,512]{1,0:T(8,128)(2,1)S(1)}, bf16[512,512]{1,0:T(8,128)(2,1)}, u32[]{:S(2)}) copy-start(bf16[512,512]{1,0:T(8,128)(2,1)} %fusion.27) | copy-start | bytes 1572868
Sparse Core Ops, SparseCore 0:
  8.9 49.5 all-gather.19
  60.4 86.2 all-gather.11
  148.6 87.4 all-gather.9
  237.8 87.4 all-gather.15
  326.8 46.8 all-gather.13
  395.6 44.7 all-gather.21
  494.0 45.7 all-gather.17
